TPU v7x, 32 devices: a whole 2x2x4 slice. The times are simulated.
32 devices in a mesh: sp: 8 (over z, y), tp: 4 (over x, core).
Axes of the slice: x: 2, y: 2, z: 4, core: 2. Of those that a mesh axis runs over, the one named last changes fastest.
Arguments:
- queries: bfloat16 [2048, 1024], P('sp', 'tp'), may hold values from -8 to 8
- keys: bfloat16 [2048, 256], P('sp', 'tp'), may hold values from -6 to 6
- values: bfloat16 [2048, 256], P('sp', 'tp'), may hold values from -6 to 6
- query_gain: float32 [64], replicated, may hold values from 0.3 to 9
- key_norm_gain: float32 [64], replicated, may hold values from 0.3 to 9
- attn_gain: float32 [1024], replicated, may hold values from 0.1 to 1.9
- residual: bfloat16 [2048, 2048], P('sp', 'tp'), may hold values from -20 to 20
- out_weight: bfloat16 [1024, 2048], P(None, 'tp'), may hold values from -0.1875 to 0.1875
- ffn_gain: float32 [2048], P('tp'), may hold values from 0.1 to 1.9
- routes: int32 [2048, 4], P('sp'), may hold values from 0 to 7, all different within a row; in each aligned block of 256 rows (0 to 255, 256 to 511, ...) at most 192 rows name the same one
- route_weight: float32 [2048, 4], P('sp'), may hold values from 0.2 to 1
- gate_weight: bfloat16 [8, 2048, 2048], P('sp', None, 'tp'), may hold values from -0.5 to 0.5
- up_weight: bfloat16 [8, 2048, 2048], P('sp', None, 'tp'), may hold values from -0.5 to 0.5
- down_weight: bfloat16 [8, 2048, 2048], P('sp', 'tp'), may hold values from -0.0068359375 to 0.0068359375
Outputs:
- layer_out: bfloat16 [2048, 2048], P('sp', 'tp')
Inputs may be any that keep to these rules, and one draw needn't show every extreme that they name: Each token names 4 different experts. In the tokens of one index of sp (aligned blocks of 256 tokens) no expert is named by more than 192 routes, a bound that some block reaches.
All inputs are finite; a program needn't handle non-finite values.
Results may differ from a plain program's by a relative error of at most 0.012.
The roundings to bfloat16 on the way count: a program that leaves them out, or rounds other values in their place, can miss the bound.
Values may be sent and summed in bfloat16 or wider, within the bound.
No kernel may reach another device: no remote copies, remote signals or barrier semaphores. Data moves between devices by JAX's collectives and lax.ppermute only.
A program may use at most 64 MiB of HBM per device.

v0:
```python
import jax
import jax.numpy as jnp
from jax import lax
from jax.sharding import PartitionSpec as P

D = 2048
GRID_W = 64
EPS = 1e-06
THETA = 10000.0
ALPHA = 1.702
LIMIT = 7.0


def rotary_tables(positions, head_size, grid_width):
    row_pos = (positions // grid_width).astype(jnp.float32)
    col_pos = (positions % grid_width).astype(jnp.float32)
    half_size = head_size // 2
    inverse = THETA ** (-jnp.arange(0, half_size, 2, dtype=jnp.float32) / half_size)
    angles = jnp.concatenate([row_pos[:, None] * inverse, col_pos[:, None] * inverse], axis=-1)
    return (jnp.cos(angles), jnp.sin(angles))


def normalize_then_rotate(head_rows, gain_vector, cosine_lookup, sine_lookup):
    values_f = head_rows.astype(jnp.float32)
    scaled = (
        values_f
        * lax.rsqrt(jnp.mean(values_f * values_f, axis=-1, keepdims=True) + EPS)
        * gain_vector
    )
    first_half, second_half = jnp.split(scaled, 2, axis=-1)
    cos_part = cosine_lookup[:, None, :]
    sin_part = sine_lookup[:, None, :]
    return jnp.concatenate(
        [
            first_half * cos_part - second_half * sin_part,
            first_half * sin_part + second_half * cos_part,
        ],
        axis=-1,
    ).astype(jnp.bfloat16)


def clamped_unit(gate_sum, up_sum):
    gate_sum = jnp.minimum(gate_sum, LIMIT)
    up_sum = jnp.clip(up_sum, -LIMIT, LIMIT)
    return ((up_sum + 1.0) * gate_sum * jax.nn.sigmoid(ALPHA * gate_sum)).astype(jnp.bfloat16)


def per_device(
    queries,
    keys,
    values,
    query_gain,
    key_norm_gain,
    attn_gain,
    residual,
    out_weight,
    ffn_gain,
    routes,
    route_weight,
    gate_weight,
    up_weight,
    down_weight,
):
    tokens = queries.shape[0]
    head_size = query_gain.shape[0]
    kv_local = keys.shape[1] // head_size
    q_local = queries.shape[1] // head_size
    group_width = q_local // kv_local
    first_token = lax.axis_index("sp") * tokens
    positions = first_token + jnp.arange(tokens, dtype=jnp.int32)
    cosine_lookup, sine_lookup = rotary_tables(positions, head_size, GRID_W)
    query_rotated = normalize_then_rotate(
        queries.reshape(tokens, q_local, head_size), query_gain, cosine_lookup, sine_lookup
    )
    key_rotated = normalize_then_rotate(
        keys.reshape(tokens, kv_local, head_size), key_norm_gain, cosine_lookup, sine_lookup
    )
    query_rows = query_rotated.reshape(tokens, kv_local, group_width, head_size).transpose(
        1, 0, 2, 3
    )
    query_rows = query_rows.reshape(kv_local, tokens * group_width, head_size)
    value_rows = values.reshape(tokens, kv_local, head_size)
    score_scale = head_size ** (-0.5)
    query_width = tokens * group_width
    start_state = (
        jnp.full((kv_local, query_width), -1e30, jnp.float32),
        jnp.zeros((kv_local, query_width), jnp.float32),
        jnp.zeros((kv_local, query_width, head_size), jnp.float32),
    )
    piece_keys = lax.all_gather(key_rotated, "sp", axis=0, tiled=True)
    piece_values = lax.all_gather(value_rows, "sp", axis=0, tiled=True)
    slot_count = piece_keys.shape[0]
    block_rows = 2048
    key_blocks = piece_keys.reshape(slot_count // block_rows, block_rows, kv_local, head_size)
    value_blocks = piece_values.reshape(slot_count // block_rows, block_rows, kv_local, head_size)

    def one_block(softmax_state, pair_block):
        running_max, running_sum, accumulated = softmax_state
        key_block, value_block = pair_block
        scores = (
            jnp.einsum("kqd,nkd->kqn", query_rows, key_block, preferred_element_type=jnp.float32)
            * score_scale
        )
        new_max = jnp.maximum(running_max, jnp.max(scores, axis=-1))
        weights = jnp.exp(scores - new_max[..., None])
        factor = jnp.exp(running_max - new_max)
        running_sum = running_sum * factor + jnp.sum(weights, axis=-1)
        accumulated = accumulated * factor[..., None] + jnp.einsum(
            "kqn,nkd->kqd",
            weights.astype(jnp.bfloat16),
            value_block,
            preferred_element_type=jnp.float32,
        )
        return ((new_max, running_sum, accumulated), None)

    final_state, unused_out = lax.scan(one_block, start_state, (key_blocks, value_blocks))
    running_max, running_sum, accumulated = final_state
    attended = (accumulated / running_sum[..., None]).reshape(
        kv_local, tokens, group_width, head_size
    )
    attended = (
        attended.transpose(1, 0, 2, 3).reshape(tokens, q_local * head_size).astype(jnp.bfloat16)
    )
    all_heads = lax.all_gather(attended, "tp", axis=1, tiled=True)
    head_f = all_heads.astype(jnp.float32)
    attn_normed = (
        head_f * lax.rsqrt(jnp.mean(head_f * head_f, axis=-1, keepdims=True) + EPS) * attn_gain
    ).astype(jnp.bfloat16)
    mid_stream = (
        residual.astype(jnp.float32)
        + jnp.dot(attn_normed, out_weight, preferred_element_type=jnp.float32)
    ).astype(jnp.bfloat16)
    mid_f = mid_stream.astype(jnp.float32)
    square_total = lax.psum(jnp.sum(mid_f * mid_f, axis=-1), "tp")
    ffn_in = (mid_f * lax.rsqrt(square_total / D + EPS)[:, None] * ffn_gain).astype(jnp.bfloat16)
    experts = lax.axis_size("sp")
    top_k = routes.shape[1]
    capacity = tokens * top_k * 3 // (2 * experts)
    route_list = routes.reshape(-1)
    onehot = (route_list[:, None] == jnp.arange(experts, dtype=jnp.int32)[None, :]).astype(
        jnp.int32
    )
    route_ranks = jnp.sum((jnp.cumsum(onehot, axis=0) - 1) * onehot, axis=1)
    slot_index = route_list * capacity + route_ranks
    slot_owner = (
        jnp.full((experts * capacity,), tokens, jnp.int32)
        .at[slot_index]
        .set(jnp.arange(tokens * top_k, dtype=jnp.int32) // top_k)
    )
    padded = jnp.concatenate([ffn_in, jnp.zeros((1, ffn_in.shape[1]), ffn_in.dtype)], axis=0)
    slot_block = lax.all_to_all(
        padded[slot_owner].reshape(experts, capacity, ffn_in.shape[1]),
        "sp",
        split_axis=0,
        concat_axis=0,
        tiled=True,
    )
    slot_count = slot_block.shape[1]
    slot_rows = slot_block.reshape(-1, slot_block.shape[2])
    column_piece = lax.all_gather(slot_rows, "tp", axis=1, tiled=True)
    gate_rows = gate_weight[0]
    up_rows = up_weight[0]
    gate_sum = jnp.dot(column_piece, gate_rows, preferred_element_type=jnp.float32)
    up_sum = jnp.dot(column_piece, up_rows, preferred_element_type=jnp.float32)
    partial_value = jnp.dot(
        clamped_unit(gate_sum, up_sum), down_weight[0], preferred_element_type=jnp.float32
    )
    summed = lax.psum_scatter(
        partial_value.astype(jnp.bfloat16), "tp", scatter_dimension=1, tiled=True
    )
    results = lax.all_to_all(
        summed.reshape(experts, slot_count, summed.shape[1]),
        "sp",
        split_axis=0,
        concat_axis=0,
        tiled=True,
    )
    picked = results.reshape(experts * capacity, -1)[slot_index].astype(jnp.float32)
    weighted = jnp.sum(
        (picked * route_weight.reshape(-1)[:, None]).reshape(tokens, top_k, -1), axis=1
    )
    return (mid_f + weighted).astype(jnp.bfloat16)


def solution(mesh):
    placed = (
        P("sp", "tp"),
        P("sp", "tp"),
        P("sp", "tp"),
        P(),
        P(),
        P(),
        P("sp", "tp"),
        P(None, "tp"),
        P("tp"),
        P("sp", None),
        P("sp", None),
        P("sp", None, "tp"),
        P("sp", None, "tp"),
        P("sp", "tp", None),
    )
    return jax.shard_map(
        per_device, mesh=mesh, in_specs=placed, out_specs=P("sp", "tp"), check_vma=False
    )
```

profile of v0, /device:TPU:0, one launch (start us, length us, event | category | flops | bytes accessed | tf_op | source)
XLA Modules:
  0.0 336.8 jit_solution(17960513029377368136)
XLA Ops:
  6.6 1.0 copy.29
  7.5 0.1 eq.31
  7.6 0.1 eq.27
  7.8 0.7 broadcast_multiply_fusion.2
  8.5 1.0 copy.24
  9.5 0.1 fusion.47
  9.6 0.1 fusion.46
  9.8 0.7 fusion.31
  10.5 0.2 copy.25
  10.7 0.2 copy.26
  10.9 0.8 fusion.37
  11.7 0.8 fusion.39
  12.6 0.1 subtract_convert_fusion.1
  12.7 32.6 %all_gather.12 = bf16[2048,1,64]{0,2,1:T(8,128)(2,1)S(1)} all-gather(bf16[256,1,64]{0,2,1:T(8,128)(2,1)S(1)} %pad_maximum_fusion.2), channel_id=1, replica_groups=mesh['sp'=8,'tp'=4] {'sp'}, dimensions={0}, use_global_device_ids=true | all-gather | bytes 294912 | tf_op jit(solution)/shard_map/all_gather | solution.py:90
  45.3 1.4 multiply_reduce_fusion
  46.7 1.9 fusion
  48.6 30.7 %all-gather = bf16[2048,64]{0,1:T(8,128)(2,1)S(1)} all-gather(bf16[256,64]{0,1:T(8,128)(2,1)S(1)} %copy-done.2), channel_id=2, replica_groups=mesh['sp'=8,'tp'=4] {'sp'}, dimensions={0}, use_global_device_ids=true | all-gather | bytes 294912 | tf_op jit(solution)/shard_map/all_gather | solution.py:91
  79.4 1.7 fusion.19
  81.0 0.2 copy.27
  81.2 0.2 convert_element_type.94
  81.4 7.2 %all_gather.14 = bf16[256,1024]{1,0:T(8,128)(2,1)S(1)} all-gather(bf16[256,256]{1,0:T(8,128)(2,1)S(1)} %convert_element_type.94), channel_id=1, replica_groups=mesh['sp'=8,'tp'=4] {'tp'}, dimensions={1}, use_global_device_ids=true | all-gather | bytes 655360 | tf_op jit(solution)/shard_map/all_gather | solution.py:124
  88.6 0.2 fusion.22
  88.8 1.8 multiply_reduce_fusion.2
  90.6 6.4 %psum.7 = f32[256]{0:T(256)S(1)} all-reduce(f32[256]{0:T(256)S(1)} %get-tuple-element.42), channel_id=1, replica_groups=mesh['sp'=8,'tp'=4] {'tp'}, use_global_device_ids=true, to_apply=%region_6.7 | all-reduce | flops 256 | bytes 2048 | tf_op jit(solution)/shard_map/psum | solution.py:134
  97.1 2.3 reduce-window.6
  99.3 0.3 slice_reduce_fusion
  99.6 0.2 reduce-window.9
  99.8 0.1 add_bitcast_fusion
  99.9 0.1 copy.28
  100.0 0.1 mul.289
  100.2 4.3 %scatter_custom_fusion = s32[1536]{0:T(1024)S(1)} fusion(s32[1024]{0:T(1024)S(1)} %bitcast.59, s32[1024]{0:T(1024)S(1)} %add_select_fusion, s32[]{:T(128)} %constant.98.clone.1), kind=kCustom, calls=%fused_computation.81 | custom fusion | bytes 6148 | tf_op jit(solution)/shard_map/scatter | solution.py:148
  104.5 0.1 multiply_convert_fusion
  104.7 5.4 %gather_fusion = bf16[1536,512]{1,0:T(8,128)(2,1)} fusion(bf16[257,512]{1,0:T(8,128)(2,1)S(1)} %concatenate.58, s32[2048]{0:T(1024)S(1)} %pad_clamp_fusion), kind=kCustom, calls=%fused_computation | custom fusion | bytes 3151872 | tf_op jit(solution)/shard_map/gather | solution.py:152
  110.1 42.0 %all_to_all.10 = bf16[8,192,512]{2,1,0:T(8,128)(2,1)} all-to-all(bf16[8,192,512]{2,1,0:T(8,128)(2,1)} %bitcast.54), channel_id=1, replica_groups=mesh['sp'=8,'tp'=4] {'sp'}, dimensions={0} | all-to-all | bytes 3145728 | tf_op jit(solution)/shard_map/all_to_all | solution.py:151
  152.1 0.0 all-gather.3.cloned.1.call-update
  152.1 0.2 reduce-scatter.2.cloned.1.call-start
  152.4 44.6 %all-gather.3.cloned.1.call-done = bf16[1536,2048]{1,0:T(8,128)(2,1)} async-done(((bf16[1536,512]{1,0:T(8,128)(2,1)}), bf16[1536,2048]{1,0:T(8,128)(2,1)}) %all-gather.3.cloned.1.call-update) | async-done | bytes 6291472 | tf_op jit(solution)/shard_map/all_gather | solution.py:160
  197.0 8.5 %convolution_minimum_fusion = f32[1536,512]{1,0:T(8,128)} fusion(bf16[1536,2048]{1,0:T(8,128)(2,1)} %all-gather.3.cloned.1.call-done, bf16[1,2048,512]{2,1,0:T(8,128)(2,1)} %param.25), kind=kOutput, calls=%fused_computation.10 | convolution fusion | flops 3222011904 | bytes 11534336 | tf_op jit(solution)/shard_map/dot_general | solution.py:163
  205.5 11.9 %convolution_convert_fusion = bf16[1536,2048]{1,0:T(8,128)(2,1)} fusion(bf16[1,512,2048]{2,1,0:T(8,128)(2,1)S(1)} %copy-done, f32[1536,512]{1,0:T(8,128)} %convolution_minimum_fusion, bf16[1536,2048]{1,0:T(8,128)(2,1)} %all-gather.3.cloned.1.call-done, bf16[1,2048,512]{2,1,0:T(8,128)(2,1)} %param.26), kind=kOutput, calls=%fused_computation.5 | convolution fusion | flops 6452674560 | bytes 19922944 | tf_op jit(solution)/shard_map/dot_general | solution.py:165
  217.4 0.0 reduce-scatter.2.cloned.1.call-update
  217.4 58.0 %reduce-scatter.2.cloned.1.call-done = bf16[1536,512]{1,0:T(8,128)(2,1)} async-done(((bf16[1536,2048]{1,0:T(8,128)(2,1)}), bf16[1536,512]{1,0:T(8,128)(2,1)}) %reduce-scatter.2.cloned.1.call-update) | async-done | bytes 1572880 | tf_op jit(solution)/shard_map/reduce_scatter | solution.py:168
  275.4 5.5 %all-to-all-start.1 = ((bf16[8,192,512]{2,1,0:T(8,128)(2,1)}), bf16[8,192,512]{2,1,0:T(8,128)(2,1)}, u32[]{:S(2)}, u32[]{:S(2)}) async-start(bf16[8,192,512]{2,1,0:T(8,128)(2,1)} %bitcast.55), calls=%async_computation.2 | async-start | bytes 3145728 | tf_op jit(solution)/shard_map/all_to_all | solution.py:171
  281.0 0.1 copy.31
  281.1 36.8 %all-to-all-done.1 = bf16[8,192,512]{2,1,0:T(8,128)(2,1)} async-done(((bf16[8,192,512]{2,1,0:T(8,128)(2,1)}), bf16[8,192,512]{2,1,0:T(8,128)(2,1)}, u32[]{:S(2)}, u32[]{:S(2)}) %all-to-all-start.1) | async-done | bytes 1572896 | tf_op jit(solution)/shard_map/all_to_all | solution.py:171
  317.9 5.6 %gather_fusion.1 = bf16[1024,512]{1,0:T(8,128)(2,1)S(1)} fusion(bf16[1536,512]{1,0:T(8,128)(2,1)} %bitcast.17, s32[1024]{0:T(1024)S(1)} %broadcast_clamp_fusion), kind=kCustom, calls=%fused_computation.1 | custom fusion | bytes 2101248 | tf_op jit(solution)/shard_map/gather | solution.py:178
  323.5 1.7 reshape.401
  325.2 2.9 multiply_reduce_fusion.1
  328.2 1.8 add_convert_fusion
  (34 shorter events, 0.3 us)
Async XLA Ops:
  6.5 199.0 %copy-start = (bf16[1,512,2048]{2,1,0:T(8,128)(2,1)S(1)}, bf16[1,512,2048]{2,1,0:T(8,128)(2,1)}, u32[]{:S(2)}) copy-start(bf16[1,512,2048]{2,1,0:T(8,128)(2,1)} %param.27) | copy-start | bytes 6291460
  6.5 190.4 %all-gather.3.cloned.1.call-start = ((), (), s32[]{:S(2)}) async-start(), calls=%async_computation.3 | async-start | bytes 7864320 | tf_op jit(solution)/shard_map/all_gather | solution.py:160
  46.7 2.0 copy-start.2
  79.4 9.4 %copy-start.5 = (bf16[256,512]{1,0:T(8,128)(2,1)S(1)}, bf16[256,512]{1,0:T(8,128)(2,1)}, u32[]{:S(2)}) copy-start(bf16[256,512]{1,0:T(8,128)(2,1)} %param.20) | copy-start | bytes 786436
  79.4 9.4 %copy-start.6 = (f32[1024]{0:T(1024)S(1)}, f32[1024]{0:T(1024)}, u32[]{:S(2)}) copy-start(f32[1024]{0:T(1024)} %param.19) | copy-start | bytes 12292
  81.0 23.5 %copy-start.4 = (f32[512]{0:T(512)S(1)}, f32[512]{0:T(512)}, u32[]{:S(2)}) copy-start(f32[512]{0:T(512)} %param.22) | copy-start | bytes 6148
  90.6 13.9 %copy-start.1 = (f32[256,512]{1,0:T(8,128)}, f32[256,512]{1,0:T(8,128)S(1)}, u32[]{:S(2)}) copy-start(f32[256,512]{1,0:T(8,128)S(1)} %get-tuple-element.43) | copy-start | bytes 1572868
  152.1 123.3 %reduce-scatter.2.cloned.1.call-start = ((), (), s32[]{:S(2)}) async-start(), calls=%async_computation.4 | async-start | bytes 7864320 | tf_op jit(solution)/shard_map/reduce_scatter | solution.py:168
  217.4 63.6 %copy-start.3 = (f32[256,4]{0,1:T(4,128)S(1)}, f32[256,4]{0,1:T(4,128)}, u32[]{:S(2)}) copy-start(f32[256,4]{0,1:T(4,128)} %param.24) | copy-start | bytes 12292
  275.4 42.4 %all-to-all-start.1 = ((bf16[8,192,512]{2,1,0:T(8,128)(2,1)}), bf16[8,192,512]{2,1,0:T(8,128)(2,1)}, u32[]{:S(2)}, u32[]{:S(2)}) async-start(bf16[8,192,512]{2,1,0:T(8,128)(2,1)} %bitcast.55), calls=%async_computation.2 | async-start | bytes 3145728 | tf_op jit(solution)/shard_map/all_to_all | solution.py:171
Sparse Core Ops, SparseCore 0:
  152.3 44.6 all-gather.2
  217.5 57.8 reduce-scatter.1
where the time goes:
time: 337 us
  waiting for transfers between devices  139 us (41%)
  blocking collectives  119 us (35%)
  matrix products  25.2 us (7%)
  local copies, waits for them, and re-layouts  20.7 us (6%)
  between operations  13.7 us (4%)
  other arithmetic  13.1 us (4%)
  starting transfers between devices  5.74 us (2%)
    reduce_scatter x1, waiting for transfers between devices, per_device(): lax.psum_scatter(partial_value.astype(jnp.bfloat16), 'tp', scatter_dimens...  58 us
    all_gather x1, waiting for transfers between devices, per_device(): column_piece = lax.all_gather(slot_rows, 'tp', axis=1, tiled=True)  44.6 us
    all_to_all x1, blocking collectives, per_device(): lax.all_to_all(padded[slot_owner].reshape(experts, capacity, ffn_in.shape...  42 us
    all_to_all x1, waiting for transfers between devices, per_device(): lax.all_to_all(summed.reshape(experts, slot_count, summed.shape[1]), 'sp'...  36.8 us
    all_gather x1, blocking collectives, per_device(): piece_keys = lax.all_gather(key_rotated, 'sp', axis=0, tiled=True)  32.6 us
    all_gather x1, blocking collectives, per_device(): piece_values = lax.all_gather(value_rows, 'sp', axis=0, tiled=True)  30.7 us
    dot_general x1, matrix products, per_device(): jnp.dot(clamped_unit(gate_sum, up_sum), down_weight[0], preferred_element...  11.9 us
    dot_general x1, matrix products, per_device(): jnp.dot(column_piece, gate_rows, preferred_element_type=jnp.float32)  8.52 us
  transfers between devices with their start and end apart: 3, of which 3 were waited for; matrix products, arithmetic and copies ran while one was open for 0% of the time, Pallas kernels for 0%

commit v1 on v0

--- a/solution.py
+++ b/solution.py
@@ -157,7 +157,12 @@
     )
     slot_count = slot_block.shape[1]
     slot_rows = slot_block.reshape(-1, slot_block.shape[2])
-    column_piece = lax.all_gather(slot_rows, "tp", axis=1, tiled=True)
+    ring = [slot_rows]
+    for hop in range(3):
+        ring.append(lax.ppermute(ring[-1], "tp", [(dev, (dev + 1) % 4) for dev in range(4)]))
+    column_piece = jnp.roll(
+        jnp.concatenate(ring[::-1], axis=1), (lax.axis_index("tp") + 1) * ring[0].shape[1], axis=1
+    )
     gate_rows = gate_weight[0]
     up_rows = up_weight[0]
     gate_sum = jnp.dot(column_piece, gate_rows, preferred_element_type=jnp.float32)

time: 337 us -> 362 us (1.074)
  local copies, waits for them, and re-layouts: 20.7 us -> 35.1 us
  waiting for transfers between devices: 139 us -> 153 us
    ppermute x0 -> x3, waiting for transfers between devices: none -> 59.9 us  [per_device(): lax.ppermute(ring[-1], 'tp', [(dev, (dev + 1) % 4) for dev in range(4)])]
    all_gather x1 -> x0, waiting for transfers between devices: 44.6 us -> none  [per_device(): column_piece = lax.all_gather(slot_rows, 'tp', axis=1, tiled=True)]
    unnamed x17 -> x36, local copies, waits for them, and re-layouts: 2.13 us -> 16.3 us
  transfers between devices with their start and end apart: 3 -> 5, of which waited for: 3 -> 5; matrix products, arithmetic and copies ran while one was open for 0% -> 0% of each run, Pallas kernels for 0% -> 0%
where the time goes in v1:
time: 362 us; the launch traced here: 361 us
  waiting for transfers between devices  153 us (42%)
  blocking collectives  119 us (33%)
  local copies, waits for them, and re-layouts  35.1 us (10%)
  matrix products  21.9 us (6%)
  between operations  13.8 us (4%)
  other arithmetic  13.1 us (4%)
  starting transfers between devices  5.52 us (2%)
    ppermute x3, waiting for transfers between devices, per_device(): lax.ppermute(ring[-1], 'tp', [(dev, (dev + 1) % 4) for dev in range(4)])  59.9 us
    reduce_scatter x1, waiting for transfers between devices, per_device(): lax.psum_scatter(partial_value.astype(jnp.bfloat16), 'tp', scatter_dimens...  56.3 us
    all_to_all x1, blocking collectives, per_device(): lax.all_to_all(padded[slot_owner].reshape(experts, capacity, ffn_in.shape...  41.9 us
    all_to_all x1, waiting for transfers between devices, per_device(): lax.all_to_all(summed.reshape(experts, slot_count, summed.shape[1]), 'sp'...  36.8 us
    all_gather x1, blocking collectives, per_device(): piece_keys = lax.all_gather(key_rotated, 'sp', axis=0, tiled=True)  32.6 us
    all_gather x1, blocking collectives, per_device(): piece_values = lax.all_gather(value_rows, 'sp', axis=0, tiled=True)  30.7 us
    unnamed x36, local copies, waits for them, and re-layouts  16.3 us
    dot_general x1, matrix products, per_device(): jnp.dot(clamped_unit(gate_sum, up_sum), down_weight[0], preferred_element...  11.9 us
  transfers between devices with their start and end apart: 5, of which 5 were waited for; matrix products, arithmetic and copies ran while one was open for 0% of the time, Pallas kernels for 0%

profile of v1, /device:TPU:0, one launch (start us, length us, event | category | flops | bytes accessed | tf_op | source)
XLA Modules:
  0.0 361.3 jit_solution(5351138329881224043)
XLA Ops:
  6.6 1.0 copy.29
  7.8 0.7 broadcast_multiply_fusion.2
  8.5 1.0 copy.24
  9.8 0.7 fusion.51
  10.5 0.2 copy.25
  10.7 0.2 copy.26
  10.9 0.8 fusion.57
  11.7 0.8 fusion.59
  12.7 32.6 %all_gather.9 = bf16[2048,1,64]{0,2,1:T(8,128)(2,1)S(1)} all-gather(bf16[256,1,64]{0,2,1:T(8,128)(2,1)S(1)} %pad_maximum_fusion.2), channel_id=1, replica_groups=mesh['sp'=8,'tp'=4] {'sp'}, dimensions={0}, use_global_device_ids=true | all-gather | bytes 294912 | tf_op jit(solution)/shard_map/all_gather | solution.py:90
  45.3 1.4 multiply_reduce_fusion
  46.7 1.9 fusion
  48.6 30.7 %all-gather = bf16[2048,64]{0,1:T(8,128)(2,1)S(1)} all-gather(bf16[256,64]{0,1:T(8,128)(2,1)S(1)} %copy-done.7), channel_id=2, replica_groups=mesh['sp'=8,'tp'=4] {'sp'}, dimensions={0}, use_global_device_ids=true | all-gather | bytes 294912 | tf_op jit(solution)/shard_map/all_gather | solution.py:91
  79.4 1.7 fusion.41
  81.0 0.2 copy.27
  81.2 0.2 convert_element_type.94
  81.4 7.2 %all_gather.11 = bf16[256,1024]{1,0:T(8,128)(2,1)S(1)} all-gather(bf16[256,256]{1,0:T(8,128)(2,1)S(1)} %convert_element_type.94), channel_id=1, replica_groups=mesh['sp'=8,'tp'=4] {'tp'}, dimensions={1}, use_global_device_ids=true | all-gather | bytes 655360 | tf_op jit(solution)/shard_map/all_gather | solution.py:124
  88.6 0.2 fusion.44
  88.8 1.8 multiply_reduce_fusion.2
  90.6 6.4 %psum.7 = f32[256]{0:T(256)S(1)} all-reduce(f32[256]{0:T(256)S(1)} %get-tuple-element.42), channel_id=1, replica_groups=mesh['sp'=8,'tp'=4] {'tp'}, use_global_device_ids=true, to_apply=%region_6.7 | all-reduce | flops 256 | bytes 2048 | tf_op jit(solution)/shard_map/psum | solution.py:134
  97.1 2.3 reduce-window.6
  99.3 0.3 slice_reduce_fusion
  99.6 0.2 reduce-window.9
  100.2 4.3 %scatter_custom_fusion = s32[1536]{0:T(1024)S(1)} fusion(s32[1024]{0:T(1024)S(1)} %bitcast.59, s32[1024]{0:T(1024)S(1)} %add_select_fusion, s32[]{:T(128)} %constant.120.clone.1), kind=kCustom, calls=%fused_computation.93 | custom fusion | bytes 6148 | tf_op jit(solution)/shard_map/scatter | solution.py:148
  104.7 5.4 %gather_fusion = bf16[1536,512]{1,0:T(8,128)(2,1)} fusion(bf16[257,512]{1,0:T(8,128)(2,1)S(1)} %concatenate.64, s32[2048]{0:T(1024)S(1)} %pad_clamp_fusion), kind=kCustom, calls=%fused_computation | custom fusion | bytes 3151872 | tf_op jit(solution)/shard_map/gather | solution.py:152
  110.1 41.9 %all_to_all.10 = bf16[8,192,512]{2,1,0:T(8,128)(2,1)S(1)} all-to-all(bf16[8,192,512]{2,1,0:T(8,128)(2,1)} %bitcast.54), channel_id=1, replica_groups=mesh['sp'=8,'tp'=4] {'sp'}, dimensions={0} | all-to-all | bytes 3145728 | tf_op jit(solution)/shard_map/all_to_all | solution.py:151
  152.0 1.1 copy-done.1
  153.2 19.8 %collective-permute-done = bf16[1536,512]{1,0:T(8,128)(2,1)S(1)} collective-permute-done((bf16[1536,512]{1,0:T(8,128)(2,1)S(1)}, bf16[1536,512]{1,0:T(8,128)(2,1)S(1)}, u32[]{:S(2)}, u32[]{:S(2)}) %collective-permute-start) | collective-permute-done | bytes 1572896 | tf_op jit(solution)/shard_map/ppermute | solution.py:162
  173.0 1.2 copy-done.3
  174.2 19.9 %collective-permute-done.1 = bf16[1536,512]{1,0:T(8,128)(2,1)} collective-permute-done((bf16[1536,512]{1,0:T(8,128)(2,1)S(1)}, bf16[1536,512]{1,0:T(8,128)(2,1)}, u32[]{:S(2)}, u32[]{:S(2)}) %collective-permute-start.1) | collective-permute-done | bytes 1572896 | tf_op jit(solution)/shard_map/ppermute | solution.py:162
  194.1 20.2 %collective-permute-done.2 = bf16[1536,512]{1,0:T(8,128)(2,1)} collective-permute-done((bf16[1536,512]{1,0:T(8,128)(2,1)}, bf16[1536,512]{1,0:T(8,128)(2,1)}, u32[]{:S(2)}, u32[]{:S(2)}) %collective-permute-start.2) | collective-permute-done | bytes 1572896 | tf_op jit(solution)/shard_map/ppermute | solution.py:162
  214.3 1.6 constant_dynamic-update-slice_fusion.7
  215.9 1.8 constant_dynamic-update-slice_fusion.6
  217.7 0.2 constant_dynamic-update-slice_fusion.5
  217.9 0.2 constant_dynamic-update-slice_fusion.4
  218.1 1.6 constant_dynamic-update-slice_fusion.3
  219.8 1.6 constant_dynamic-update-slice_fusion.2
  221.4 0.2 constant_dynamic-update-slice_fusion.1
  221.6 0.2 constant_dynamic-update-slice_fusion
  221.8 4.6 %copy-done.6 = bf16[1536,4096]{1,0:T(8,128)(2,1)} copy-done((bf16[1536,4096]{1,0:T(8,128)(2,1)}, bf16[1536,4096]{1,0:T(8,128)(2,1)S(1)}, u32[]{:S(2)}) %copy-start.6) | copy-done | bytes 12582936
  226.4 5.2 %fusion.11 = f32[1536,512]{1,0:T(8,128)} fusion(bf16[1536,4096]{1,0:T(8,128)(2,1)S(1)} %constant_dynamic-update-slice_fusion, s32[]{:T(128)S(6)} %select_n.57, bf16[1,2048,512]{2,1,0:T(8,128)(2,1)S(1)} %copy-done.10), kind=kOutput, calls=%fused_computation.14 | convolution fusion | flops 3222011904 | bytes 11534340 | tf_op jit(solution)/shard_map/dot_general | solution.py:168
  231.6 11.9 %convolution_convert_fusion = bf16[1536,2048]{1,0:T(8,128)(2,1)} fusion(bf16[1,512,2048]{2,1,0:T(8,128)(2,1)S(1)} %copy-done, f32[1536,512]{1,0:T(8,128)} %fusion.11, bf16[1536,4096]{1,0:T(8,128)(2,1)} %copy-done.6, s32[]{:T(128)S(6)} %select_n.57, bf16[1,2048,512]{2,1,0:T(8,128)(2,1)} %param.26), kind=kOutput, calls=%fused_computation.5 | convolution fusion | flops 6452674560 | bytes 19922948 | tf_op jit(solution)/shard_map/dot_general | solution.py:170
  243.6 56.3 %reduce-scatter.2.cloned.1.call-done = bf16[1536,512]{1,0:T(8,128)(2,1)} async-done(((bf16[1536,2048]{1,0:T(8,128)(2,1)}), bf16[1536,512]{1,0:T(8,128)(2,1)}) %reduce-scatter.2.cloned.1.call-update) | async-done | bytes 1572880 | tf_op jit(solution)/shard_map/reduce_scatter | solution.py:173
  299.9 5.5 %all-to-all-start.1 = ((bf16[8,192,512]{2,1,0:T(8,128)(2,1)}), bf16[8,192,512]{2,1,0:T(8,128)(2,1)}, u32[]{:S(2)}, u32[]{:S(2)}) async-start(bf16[8,192,512]{2,1,0:T(8,128)(2,1)} %bitcast.55), calls=%async_computation.2 | async-start | bytes 3145728 | tf_op jit(solution)/shard_map/all_to_all | solution.py:176
  305.6 36.8 %all-to-all-done.1 = bf16[8,192,512]{2,1,0:T(8,128)(2,1)} async-done(((bf16[8,192,512]{2,1,0:T(8,128)(2,1)}), bf16[8,192,512]{2,1,0:T(8,128)(2,1)}, u32[]{:S(2)}, u32[]{:S(2)}) %all-to-all-start.1) | async-done | bytes 1572896 | tf_op jit(solution)/shard_map/all_to_all | solution.py:176
  342.4 5.6 %gather_fusion.1 = bf16[1024,512]{1,0:T(8,128)(2,1)S(1)} fusion(bf16[1536,512]{1,0:T(8,128)(2,1)} %bitcast.17, s32[1024]{0:T(1024)S(1)} %broadcast_clamp_fusion), kind=kCustom, calls=%fused_computation.1 | custom fusion | bytes 2101248 | tf_op jit(solution)/shard_map/gather | solution.py:183
  348.0 1.7 reshape.401
  349.7 2.9 multiply_reduce_fusion.1
  352.6 1.8 add_convert_fusion
  (57 shorter events, 1.5 us)
Async XLA Ops:
  6.5 225.1 %copy-start = (bf16[1,512,2048]{2,1,0:T(8,128)(2,1)S(1)}, bf16[1,512,2048]{2,1,0:T(8,128)(2,1)}, u32[]{:S(2)}) copy-start(bf16[1,512,2048]{2,1,0:T(8,128)(2,1)} %param.27) | copy-start | bytes 6291460
  6.5 293.3 %reduce-scatter.2.cloned.1.call-start = ((), (), s32[]{:S(2)}) async-start(), calls=%async_computation.3 | async-start | bytes 7864320 | tf_op jit(solution)/shard_map/reduce_scatter | solution.py:173
  46.7 2.0 copy-start.7
  79.4 9.4 %copy-start.11 = (bf16[256,512]{1,0:T(8,128)(2,1)S(1)}, bf16[256,512]{1,0:T(8,128)(2,1)}, u32[]{:S(2)}) copy-start(bf16[256,512]{1,0:T(8,128)(2,1)} %param.20) | copy-start | bytes 786436
  79.4 9.4 %copy-start.12 = (f32[1024]{0:T(1024)S(1)}, f32[1024]{0:T(1024)}, u32[]{:S(2)}) copy-start(f32[1024]{0:T(1024)} %param.19) | copy-start | bytes 12292
  81.0 23.5 %copy-start.9 = (f32[512]{0:T(512)S(1)}, f32[512]{0:T(512)}, u32[]{:S(2)}) copy-start(f32[512]{0:T(512)} %param.22) | copy-start | bytes 6148
  90.6 13.9 %copy-start.5 = (f32[256,512]{1,0:T(8,128)}, f32[256,512]{1,0:T(8,128)S(1)}, u32[]{:S(2)}) copy-start(f32[256,512]{1,0:T(8,128)S(1)} %get-tuple-element.43) | copy-start | bytes 1572868
  152.0 1.1 copy-start.1
  153.2 19.8 %collective-permute-start = (bf16[1536,512]{1,0:T(8,128)(2,1)S(1)}, bf16[1536,512]{1,0:T(8,128)(2,1)S(1)}, u32[]{:S(2)}, u32[]{:S(2)}) collective-permute-start(bf16[1536,512]{1,0:T(8,128)(2,1)S(1)} %bitcast.51), channel_id=1, source_target_pairs={{0,1},{1,2},{2,3},{3,0},{4,5},{5,6},{6,7},{7,4},{8,9},{9,10},{10,1... | collective-permute-start | bytes 4718600 | tf_op jit(solution)/shard_map/ppermute | solution.py:162
  173.0 1.2 copy-start.3
  174.2 19.9 %collective-permute-start.1 = (bf16[1536,512]{1,0:T(8,128)(2,1)S(1)}, bf16[1536,512]{1,0:T(8,128)(2,1)}, u32[]{:S(2)}, u32[]{:S(2)}) collective-permute-start(bf16[1536,512]{1,0:T(8,128)(2,1)S(1)} %collective-permute-done), channel_id=1, source_target_pairs={{0,1},{1,2},{2,3},{3,0},{4,5},{5,6},{6,7},{7,4},{8,9},{9,10},{10,1... | collective-permute-start | bytes 4718600 | tf_op jit(solution)/shard_map/ppermute | solution.py:162
  194.1 20.2 %collective-permute-start.2 = (bf16[1536,512]{1,0:T(8,128)(2,1)}, bf16[1536,512]{1,0:T(8,128)(2,1)}, u32[]{:S(2)}, u32[]{:S(2)}) collective-permute-start(bf16[1536,512]{1,0:T(8,128)(2,1)} %collective-permute-done.1), channel_id=1, source_target_pairs={{0,1},{1,2},{2,3},{3,0},{4,5},{5,6},{6,7},{7,4},{8,9},{9,10},{10,1... | collective-permute-start | bytes 4718600 | tf_op jit(solution)/shard_map/ppermute | solution.py:162
  194.1 23.6 %copy-start.4 = (bf16[1536,512]{1,0:T(8,128)(2,1)S(1)}, bf16[1536,512]{1,0:T(8,128)(2,1)}, u32[]{:S(2)}) copy-start(bf16[1536,512]{1,0:T(8,128)(2,1)} %copy-done.3) | copy-start | bytes 4718596
  215.9 2.0 copy-start.2
  221.4 5.0 %copy-start.10 = (bf16[1,2048,512]{2,1,0:T(8,128)(2,1)S(1)}, bf16[1,2048,512]{2,1,0:T(8,128)(2,1)}, u32[]{:S(2)}) copy-start(bf16[1,2048,512]{2,1,0:T(8,128)(2,1)} %param.25) | copy-start | bytes 6291460
  221.8 4.6 %copy-start.6 = (bf16[1536,4096]{1,0:T(8,128)(2,1)}, bf16[1536,4096]{1,0:T(8,128)(2,1)S(1)}, u32[]{:S(2)}) copy-start(bf16[1536,4096]{1,0:T(8,128)(2,1)S(1)} %constant_dynamic-update-slice_fusion) | copy-start | bytes 37748740
  243.5 61.9 %copy-start.8 = (f32[256,4]{0,1:T(4,128)S(1)}, f32[256,4]{0,1:T(4,128)}, u32[]{:S(2)}) copy-start(f32[256,4]{0,1:T(4,128)} %param.24) | copy-start | bytes 12292
  299.9 42.5 %all-to-all-start.1 = ((bf16[8,192,512]{2,1,0:T(8,128)(2,1)}), bf16[8,192,512]{2,1,0:T(8,128)(2,1)}, u32[]{:S(2)}, u32[]{:S(2)}) async-start(bf16[8,192,512]{2,1,0:T(8,128)(2,1)} %bitcast.55), calls=%async_computation.2 | async-start | bytes 3145728 | tf_op jit(solution)/shard_map/all_to_all | solution.py:176
Sparse Core Ops, SparseCore 0:
  243.7 56.1 reduce-scatter.1
